TPU v7x, 512 devices: a whole 4x8x8 slice. The times are simulated.
512 devices in a mesh: ep: 128 (over z, y, core), tp: 4 (over x).
Axes of the slice: x: 4, y: 8, z: 8, core: 2. Of those that a mesh axis runs over, the one named last changes fastest.
Arguments:
- tokens: bfloat16 [2048, 2048], P('ep'), may hold values from -6 to 6
- head_state: float32 [2048, 16, 4096], P('ep', 'tp'), may hold values from -6 to 6
- mixer_gain: float32 [2048], replicated, may hold values from 0.1 to 1.9
- w_query: bfloat16 [2048, 1024], P('ep', 'tp'), may hold values from -0.125 to 0.125
- w_key: bfloat16 [2048, 1024], P('ep', 'tp'), may hold values from -0.125 to 0.125
- w_value: bfloat16 [2048, 1024], P('ep', 'tp'), may hold values from -0.125 to 0.125
- decay_down: bfloat16 [2048, 64], replicated, may hold values from -0.125 to 0.125
- decay_up: bfloat16 [64, 1024], replicated, may hold values from -3 to 3
- decay_base: float32 [1024], P('tp'), may hold values from -4 to 0
- rate_down: bfloat16 [2048, 64], replicated, may hold values from -0.125 to 0.125
- rate_up: bfloat16 [64, 1024], replicated, may hold values from -0.75 to 0.75
- head_gain: float32 [1024], P('tp'), may hold values from 0.1 to 1.9
- w_out: bfloat16 [1024, 2048], P('tp', 'ep'), may hold values from -0.1875 to 0.1875
- expert_gain: float32 [2048], replicated, may hold values from 0.1 to 1.9
- expert_ids: int32 [2048, 2], P('ep'), may hold values from 0 to 127, all different within a row; in each aligned block of 16 rows (0 to 15, 16 to 31, ...) at most 1 rows name the same one
- route_weight: float32 [2048, 2], P('ep'), may hold values from 0.2 to 1
- w_gate: bfloat16 [128, 2048, 512], P('ep', None, 'tp'), may hold values from -0.125 to 0.125
- w_up: bfloat16 [128, 2048, 512], P('ep', None, 'tp'), may hold values from -0.125 to 0.125
- w_down: bfloat16 [128, 512, 2048], P('ep', 'tp'), may hold values from -0.25 to 0.25
Outputs:
- layer_out: bfloat16 [2048, 2048], P('ep', 'tp')
- next_state: float32 [2048, 16, 4096], P('ep', 'tp')
Inputs may be any that keep to these rules, and one draw needn't show every extreme that they name: `expert_ids`: each row names 2 different experts; among the 16 rows of one index of ep no expert is named more than 1 times, and in the rows of some indices one expert is named exactly 1 times.
All inputs are finite; a program needn't handle non-finite values.
Results may differ from a plain program's by a relative error of at most 0.015.
Values may be sent and summed in bfloat16 or wider, within the bound.
A program may use at most 64 MiB of HBM per device.

v0:
```python
import jax
import jax.numpy as jnp
from jax import lax
from jax.sharding import PartitionSpec as P

norm_eps = 1e-06
group_eps = 0.00064


def sent_together(arrays, axis, dim, along):
    widths = [a.shape[along] for a in arrays]
    both = jnp.concatenate(arrays, axis=along)
    out = lax.all_gather(both, axis, axis=dim, tiled=True)
    return tuple(jnp.split(out, [sum(widths[:k]) for k in range(1, len(widths))], axis=along))


def from_everyone(array, axis):
    copies = jnp.broadcast_to(array, (lax.axis_size(axis), *array.shape))
    return lax.all_to_all(copies, axis, split_axis=0, concat_axis=0, tiled=True)


def taken_together(array, axis):
    everything = from_everyone(array, axis)
    return jnp.sum(everything.astype(jnp.float32), axis=0)


def split_up(array, dim, peers):
    before, after = (array.shape[:dim], array.shape[dim + 1 :])
    return jnp.moveaxis(array.reshape(*before, peers, -1, *after), dim, 0)


def sum_at_owner(array, axis, dim):
    peers = lax.axis_size(axis)
    parts = lax.all_to_all(split_up(array, dim, peers), axis, 0, 0, tiled=True)
    return jnp.sum(parts.astype(jnp.float32), axis=0)


def rms_scale(activity, gain):
    widened = activity.astype(jnp.float32)
    scaled = widened * lax.rsqrt(jnp.mean(widened * widened, axis=-1, keepdims=True) + norm_eps)
    return (scaled * gain).astype(jnp.bfloat16)


def low_rank(normed, decay_down, decay_up, decay_base, rate_down, rate_up):
    decay_low = jnp.tanh(jnp.dot(normed, decay_down, preferred_element_type=jnp.float32)).astype(
        jnp.bfloat16
    )
    decay_pre = decay_base + jnp.dot(decay_low, decay_up, preferred_element_type=jnp.float32)
    decays = jnp.exp(-jnp.exp(-jax.nn.softplus(-decay_pre) - 0.5))
    rate_low = jnp.dot(normed, rate_down, preferred_element_type=jnp.float32).astype(jnp.bfloat16)
    rates = jax.nn.sigmoid(jnp.dot(rate_low, rate_up, preferred_element_type=jnp.float32))
    return (decays, rates)


def recurrence(queries, key_rows, value_rows, decays, rates, old_state, head_gain):
    row_count, head_count, _ = old_state.shape
    head_size = queries.shape[1] // head_count
    head_shape = (row_count, head_count, head_size)
    query_heads = queries.astype(jnp.float32).reshape(head_shape)
    key_heads = key_rows.astype(jnp.float32).reshape(head_shape)
    value_heads = value_rows.astype(jnp.float32).reshape(head_shape)
    decay_heads = decays.reshape(head_shape)
    rate_heads = rates.reshape(head_shape)
    unit_keys = key_heads * lax.rsqrt(jnp.sum(key_heads * key_heads, axis=-1, keepdims=True) + 1.0)
    state_grid = old_state.reshape(row_count, head_count, head_size, head_size)
    removed = jnp.sum(state_grid * unit_keys[:, :, None, :], axis=-1)
    updated = (
        state_grid * decay_heads[:, :, None, :]
        - removed[:, :, :, None] * (unit_keys * rate_heads)[:, :, None, :]
        + value_heads[:, :, :, None] * key_heads[:, :, None, :]
    )
    readout = jnp.sum(updated * query_heads[:, :, None, :], axis=-1)
    centred = readout - jnp.mean(readout, axis=-1, keepdims=True)
    spread = jnp.mean(centred * centred, axis=-1, keepdims=True)
    scaled = centred * lax.rsqrt(spread + group_eps) * head_gain.reshape(head_count, head_size)
    return (
        updated.reshape(row_count, head_count, head_size * head_size),
        scaled.reshape(row_count, head_count * head_size).astype(jnp.bfloat16),
    )


def body(
    tokens,
    head_state,
    mixer_gain,
    w_query,
    w_key,
    w_value,
    decay_down,
    decay_up,
    decay_base,
    rate_down,
    rate_up,
    head_gain,
    w_out,
    expert_gain,
    expert_ids,
    route_weight,
    w_gate,
    w_up,
    w_down,
):
    seq_rows, width = tokens.shape
    local_cols = w_query.shape[1]
    head_lane = lax.axis_index("tp")
    normed = rms_scale(tokens, mixer_gain)
    pieces = sent_together((w_query, w_key, w_value), "ep", 0, 1)
    projected = tuple(
        (
            jnp.dot(normed, weight_piece, preferred_element_type=jnp.float32)
            for weight_piece in pieces
        )
    )
    queries, key_rows, value_rows = (member.astype(jnp.bfloat16) for member in projected)
    col_offset = head_lane * local_cols
    decays, rates = low_rank(
        normed,
        decay_down,
        lax.dynamic_slice_in_dim(decay_up, col_offset, local_cols, 1),
        decay_base,
        rate_down,
        lax.dynamic_slice_in_dim(rate_up, col_offset, local_cols, 1),
    )
    next_state, head_out = recurrence(
        queries, key_rows, value_rows, decays, rates, head_state, head_gain
    )
    partial_out = jnp.dot(
        head_out,
        lax.all_gather(w_out, "ep", axis=1, tiled=True),
        preferred_element_type=jnp.float32,
    )
    mixed_out = taken_together(partial_out.astype(jnp.bfloat16), "tp").astype(jnp.float32)
    residual = (tokens.astype(jnp.float32) + mixed_out).astype(jnp.bfloat16)
    expert_in = rms_scale(residual, expert_gain)
    experts = lax.axis_size("ep")
    top_count = expert_ids.shape[1]
    slot_count = max(1, 2 * seq_rows * top_count // experts)
    slot_total = experts * slot_count
    flat_ids = expert_ids.reshape(-1)
    matches = (flat_ids[:, None] == jnp.arange(experts, dtype=jnp.int32)[None, :]).astype(jnp.int32)
    slot_rank = jnp.sum((jnp.cumsum(matches, axis=0) - 1) * matches, axis=1)
    slot_ids = (flat_ids * slot_count + slot_rank).reshape(seq_rows, top_count)
    slot_match = (
        slot_ids[:, :, None] == jnp.arange(slot_total, dtype=jnp.int32)[None, None, :]
    ).astype(jnp.float32)
    picker = jnp.sum(slot_match, axis=1).astype(jnp.bfloat16)
    outbound = jnp.einsum("ts,td->sd", picker, expert_in, preferred_element_type=jnp.float32)
    outbound = outbound.astype(jnp.bfloat16).reshape(experts, slot_count, expert_in.shape[1])
    gate_local, up_local, down_local = (w_gate[0], w_up[0], w_down[0])
    arrived = lax.all_to_all(outbound, "ep", split_axis=0, concat_axis=0, tiled=True)
    sources, held, _ = arrived.shape
    flat_rows = arrived.reshape(sources * held, width)
    gate_act = jnp.dot(flat_rows, gate_local, preferred_element_type=jnp.float32)
    up_act = jnp.dot(flat_rows, up_local, preferred_element_type=jnp.float32)
    hidden = (jax.nn.silu(gate_act) * up_act).astype(jnp.bfloat16)
    partial_rows = jnp.dot(hidden, down_local, preferred_element_type=jnp.float32).reshape(
        sources, held, width
    )
    reduced = sum_at_owner(partial_rows.astype(jnp.bfloat16), "tp", 2)
    returned = lax.all_to_all(
        reduced.astype(jnp.bfloat16), "ep", split_axis=0, concat_axis=0, tiled=True
    )
    shares = route_weight / jnp.sum(route_weight, axis=1, keepdims=True)
    combine = jnp.sum(slot_match * shares[:, :, None], axis=1)
    routed = jnp.dot(combine, returned.reshape(slot_total, -1).astype(jnp.float32))
    own_cols = routed.shape[1]
    kept = lax.dynamic_slice_in_dim(residual, head_lane * own_cols, own_cols, 1)
    layer_out = (kept.astype(jnp.float32) + routed).astype(jnp.bfloat16)
    return (layer_out, next_state)


def solution(mesh):
    return jax.shard_map(
        body,
        mesh=mesh,
        in_specs=(
            P("ep", None),
            P("ep", "tp", None),
            P(),
            P("ep", "tp"),
            P("ep", "tp"),
            P("ep", "tp"),
            P(),
            P(),
            P("tp"),
            P(),
            P(),
            P("tp"),
            P("tp", "ep"),
            P(),
            P("ep", None),
            P("ep", None),
            P("ep", None, "tp"),
            P("ep", None, "tp"),
            P("ep", "tp", None),
        ),
        out_specs=(P("ep", "tp"), P("ep", "tp", None)),
        check_vma=False,
    )
```

profile of v0, /device:TPU:1, one launch (start us, length us, event | category | flops | bytes accessed | tf_op | source)
XLA Modules:
  0.0 267.5 jit_solution(1612568220506573948)
XLA Ops:
  7.2 1.4 pad_maximum_fusion
  8.7 0.7 all-gather.5.cloned.1.call-update
  9.4 1.0 fusion.34
  10.4 1.4 fusion.10
  11.8 1.4 fusion.55
  13.4 2.1 reshape.119
  15.5 1.5 mul.201
  17.0 3.1 %mul.221 = f32[16,4,4096]{2,1,0:T(4,128)} reshape(f32[16,4,64,64]{3,2,1,0:T(8,128)} %mul.201) | data formatting | bytes 2097152 | tf_op jit(solution)/shard_map/mul | solution.py:68
  20.2 0.1 eq.28
  20.4 80.8 %all-gather.3.cloned.1.call-done = bf16[2048,768]{1,0:T(8,128)(2,1)} async-done(((bf16[16,768]{1,0:T(8,128)(2,1)}), bf16[2048,768]{1,0:T(8,128)(2,1)}) %all-gather.3.cloned.1.call-update) | async-done | bytes 3145744 | tf_op jit(solution)/shard_map/all_gather | solution.py:13
  101.2 1.5 fusion.14
  102.8 1.5 fusion.12
  104.3 0.1 reshape.130
  104.4 1.5 fusion.13
  106.0 0.1 multiply_reduce_fusion.4
  106.2 8.8 %broadcast_multiply_fusion = (f32[16,4,64,64]{3,2,1,0:T(8,128)}, f32[16,4,64]{2,1,0:T(4,128)S(1)}, f32[16,4,64,64]{3,2,1,0:T(8,128)}) fusion(f32[16,4,64]{2,1,0:T(4,128)S(1)} %reshape.128, f32[16,4,64]{2,1,0:T(4,128)S(1)} %reshape.129, f32[16,4,64]{2,1,0:T(4,128)S(1)} %reshape.130, f32[16,4,64,64]{3,2,1,0:T(8,128)S(1)} %reshape.119, ...), kind=kOutput, calls=%fused_computation.33 | output fusion | flops 2097215 | bytes 3260416 | tf_op jit(solution)/shard_map/mul | solution.py:69
  115.1 3.2 %mul.223 = f32[16,4,4096]{2,1,0:T(4,128)} reshape(f32[16,4,64,64]{3,2,1,0:T(8,128)} %get-tuple-element.12) | data formatting | bytes 2097152 | tf_op jit(solution)/shard_map/mul | solution.py:69
  118.2 1.8 mul.224
  120.1 0.1 mul.219
  120.2 1.8 mul.225
  122.0 4.1 %multiply_reduce_fusion.2 = (f32[16,4]{1,0:T(8,128)S(1)}, f32[16,4,4096]{2,1,0:T(4,128)}) fusion(f32[16,4,4096]{2,1,0:T(4,128)} %mul.225, f32[16,4,4096]{2,1,0:T(4,128)} %mul.224, f32[16,4,4096]{2,1,0:T(4,128)} %mul.223, f32[16,4,4096]{2,1,0:T(4,128)} %param.20, f32[16,4,4096]{2,1,0:T(4,128)} %mul.221), kind=kLoop, calls=%fused_computation.31 | loop fusion | flops 1310656 | bytes 6291712 | tf_op jit(solution)/shard_map/reduce_sum | solution.py:73
  126.1 0.2 multiply_reduce_fusion.3
  126.3 0.1 subtract_multiply_fusion
  126.4 0.1 mul.230
  126.5 54.1 %all-gather.5.cloned.1.call-done = bf16[256,2048]{0,1:T(8,128)(2,1)} async-done(((bf16[256,16]{0,1:T(8,128)(2,1)}), bf16[256,2048]{0,1:T(8,128)(2,1)}) %all-gather.5.cloned.1.call-update) | async-done | bytes 1048592 | tf_op jit(solution)/shard_map/all_gather | solution.py:129
  180.6 1.6 convolution_convert_fusion.2
  182.2 0.7 broadcast_in_dim.2
  182.9 4.0 %all-to-all-start = ((bf16[4,16,2048]{2,1,0:T(8,128)(2,1)}), bf16[4,16,2048]{2,1,0:T(8,128)(2,1)S(1)}, u32[]{:S(2)}, u32[]{:S(2)}) async-start(bf16[4,16,2048]{2,1,0:T(8,128)(2,1)} %broadcast_in_dim.2), calls=%async_computation | async-start | bytes 524288 | tf_op jit(solution)/shard_map/all_to_all | solution.py:19
  186.9 0.2 select_reduce_fusion.1
  187.3 5.5 %all-to-all-done = bf16[4,16,2048]{2,1,0:T(8,128)(2,1)S(1)} async-done(((bf16[4,16,2048]{2,1,0:T(8,128)(2,1)}), bf16[4,16,2048]{2,1,0:T(8,128)(2,1)S(1)}, u32[]{:S(2)}, u32[]{:S(2)}) %all-to-all-start) | async-done | bytes 262176 | tf_op jit(solution)/shard_map/all_to_all | solution.py:19
  192.8 0.1 fusion.31
  193.0 0.3 fusion.1
  193.3 0.5 broadcast.118
  193.8 1.0 reduce.4
  194.9 0.4 reshape.132
  195.2 30.2 %all_to_all.20 = bf16[128,2,1024]{2,1,0:T(2,128)(2,1)S(1)} all-to-all(bf16[128,2,1024]{2,1,0:T(2,128)(2,1)S(1)} %reshape.132), channel_id=1, replica_groups=mesh['ep'=128,'tp'=4] {'ep'}, dimensions={0} | all-to-all | bytes 1048576 | tf_op jit(solution)/shard_map/all_to_all | solution.py:150
  225.4 0.4 reshape.133
  225.9 0.4 fusion.22
  226.3 0.7 convolution_convert_fusion
  227.0 0.4 reshape.125
  227.4 0.1 copy.85
  227.5 12.2 %all_to_all.21 = bf16[4,128,1,512]{3,1,2,0:T(8,128)(2,1)S(1)} all-to-all(bf16[4,128,1,512]{3,1,2,0:T(8,128)(2,1)S(1)} %bitcast.38), channel_id=1, replica_groups=mesh['ep'=128,'tp'=4] {'tp'}, dimensions={0} | all-to-all | bytes 1048576 | tf_op jit(solution)/shard_map/all_to_all | solution.py:34
  239.8 0.7 reduce.5
  240.5 0.7 reshape.134
  241.2 5.8 %all-to-all-start.3 = ((bf16[128,2,256]{2,1,0:T(2,128)(2,1)}), bf16[128,2,256]{2,1,0:T(2,128)(2,1)S(1)}, u32[]{:S(2)}, u32[]{:S(2)}) async-start(bf16[128,2,256]{2,1,0:T(2,128)(2,1)} %reshape.134), calls=%async_computation.3 | async-start | bytes 262144 | tf_op jit(solution)/shard_map/all_to_all | solution.py:160
  247.0 12.8 %all-to-all-done.3 = bf16[128,2,256]{2,1,0:T(2,128)(2,1)S(1)} async-done(((bf16[128,2,256]{2,1,0:T(2,128)(2,1)}), bf16[128,2,256]{2,1,0:T(2,128)(2,1)S(1)}, u32[]{:S(2)}, u32[]{:S(2)}) %all-to-all-start.3) | async-done | bytes 131104 | tf_op jit(solution)/shard_map/all_to_all | solution.py:160
  259.8 0.1 reshape.135
  259.9 0.8 fusion.7
  (44 shorter events, 1.2 us)
Async XLA Ops:
  7.2 219.2 %copy-start = (bf16[1,128,2048]{2,1,0:T(8,128)(2,1)S(1)}, bf16[1,128,2048]{2,1,0:T(8,128)(2,1)}, u32[]{:S(2)}) copy-start(bf16[1,128,2048]{2,1,0:T(8,128)(2,1)} %param.37) | copy-start | bytes 1572868
  7.2 94.0 %all-gather.3.cloned.1.call-start = ((), (), s32[]{:S(2)}) async-start(), calls=%async_computation.4 | async-start | bytes 3170304 | tf_op jit(solution)/shard_map/all_gather | solution.py:13
  8.6 172.0 %all-gather.5.cloned.1.call-start = ((), (), s32[]{:S(2)}) async-start(), calls=%async_computation.5 | async-start | bytes 1056768 | tf_op jit(solution)/shard_map/all_gather | solution.py:129
  17.0 3.1 %copy-start.7 = (s32[16,2]{0,1:T(2,128)S(1)}, s32[16,2]{0,1:T(2,128)}, u32[]{:S(2)}) copy-start(s32[16,2]{0,1:T(2,128)} %param.33) | copy-start | bytes 388
  17.0 3.4 %copy-start.8 = (f32[16,2]{0,1:T(2,128)S(1)}, f32[16,2]{0,1:T(2,128)}, u32[]{:S(2)}) copy-start(f32[16,2]{0,1:T(2,128)} %param.34) | copy-start | bytes 388
  17.0 84.2 %copy-start.2 = (bf16[16,2048]{1,0:T(8,128)(2,1)S(1)}, bf16[16,2048]{1,0:T(8,128)(2,1)}, u32[]{:S(2)}) copy-start(bf16[16,2048]{1,0:T(8,128)(2,1)} %param.19) | copy-start | bytes 196612
  17.0 84.2 %copy-start.5 = (f32[2048]{0:T(1024)S(1)}, f32[2048]{0:T(1024)}, u32[]{:S(2)}) copy-start(f32[2048]{0:T(1024)} %param.21) | copy-start | bytes 24580
  115.1 3.2 %copy-start.1 = (f32[16,4,64,64]{3,2,1,0:T(8,128)S(1)}, f32[16,4,64,64]{3,2,1,0:T(8,128)}, u32[]{:S(2)}) copy-start(f32[16,4,64,64]{3,2,1,0:T(8,128)} %get-tuple-element.10) | copy-start | bytes 3145732
  122.0 58.6 %copy-start.9 = (f32[256]{0:T(256)S(1)}, f32[256]{0:T(256)}, u32[]{:S(2)}) copy-start(f32[256]{0:T(256)} %param.30) | copy-start | bytes 3076
  126.1 66.8 %copy-start.6 = (f32[2048]{0:T(1024)S(1)}, f32[2048]{0:T(1024)}, u32[]{:S(2)}) copy-start(f32[2048]{0:T(1024)} %param.32) | copy-start | bytes 24580
  182.9 9.9 %all-to-all-start = ((bf16[4,16,2048]{2,1,0:T(8,128)(2,1)}), bf16[4,16,2048]{2,1,0:T(8,128)(2,1)S(1)}, u32[]{:S(2)}, u32[]{:S(2)}) async-start(bf16[4,16,2048]{2,1,0:T(8,128)(2,1)} %broadcast_in_dim.2), calls=%async_computation | async-start | bytes 524288 | tf_op jit(solution)/shard_map/all_to_all | solution.py:19
  194.8 31.1 %copy-start.3 = (bf16[1,2048,128]{2,1,0:T(8,128)(2,1)S(1)}, bf16[1,2048,128]{2,1,0:T(8,128)(2,1)}, u32[]{:S(2)}) copy-start(bf16[1,2048,128]{2,1,0:T(8,128)(2,1)} %param.35) | copy-start | bytes 1572868
  195.2 31.1 %copy-start.4 = (bf16[1,2048,128]{2,1,0:T(8,128)(2,1)S(1)}, bf16[1,2048,128]{2,1,0:T(8,128)(2,1)}, u32[]{:S(2)}) copy-start(bf16[1,2048,128]{2,1,0:T(8,128)(2,1)} %param.36) | copy-start | bytes 1572868
  241.2 18.6 %all-to-all-start.3 = ((bf16[128,2,256]{2,1,0:T(2,128)(2,1)}), bf16[128,2,256]{2,1,0:T(2,128)(2,1)S(1)}, u32[]{:S(2)}, u32[]{:S(2)}) async-start(bf16[128,2,256]{2,1,0:T(2,128)(2,1)} %reshape.134), calls=%async_computation.3 | async-start | bytes 262144 | tf_op jit(solution)/shard_map/all_to_all | solution.py:160
Sparse Core Ops, SparseCore 0:
  11.7 89.4 all-gather.2
  104.2 76.3 all-gather.4
where the time goes:
time: 268 us; the launch traced here: 267 us
  waiting for transfers between devices  154 us (57%)
  blocking collectives  42.4 us (16%)
  other arithmetic  18.1 us (7%)
  local copies, waits for them, and re-layouts  17.9 us (7%)
  between operations  14.3 us (5%)
  matrix products  11.1 us (4%)
  starting transfers between devices  9.82 us (4%)
    all_gather x1, waiting for transfers between devices, sent_together(): out = lax.all_gather(both, axis, axis=dim, tiled=True)  80.8 us
    all_gather x1, waiting for transfers between devices, body(): lax.all_gather(w_out, 'ep', axis=1, tiled=True)  54.1 us
    all_to_all x1, blocking collectives, body(): lax.all_to_all(outbound, 'ep', split_axis=0, concat_axis=0, tiled=True)  30.2 us
    all_to_all x1, waiting for transfers between devices, body(): lax.all_to_all(reduced.astype(jnp.bfloat16), 'ep', split_axis=0, concat_a...  12.8 us
    all_to_all x1, blocking collectives, sum_at_owner(): parts = lax.all_to_all(split_up(array, dim, peers), axis, 0, 0, tiled=True)  12.2 us
    mul x1, other arithmetic, recurrence(): removed[:, :, :, None] * (unit_keys * rate_heads)[:, :, None, :]  8.83 us
    all_to_all x1, starting transfers between devices, body(): lax.all_to_all(reduced.astype(jnp.bfloat16), 'ep', split_axis=0, concat_a...  5.77 us
    all_to_all x1, waiting for transfers between devices, from_everyone(): return lax.all_to_all(copies, axis, split_axis=0, concat_axis=0, tiled=True)  5.47 us
  transfers between devices with their start and end apart: 4, of which 4 were waited for; matrix products, arithmetic and copies ran while one was open for 14% of the time, Pallas kernels for 0%

commit v1 on v0

--- a/solution.py
+++ b/solution.py
@@ -2,6 +2,7 @@
 import jax.numpy as jnp
 from jax import lax
 from jax.sharding import PartitionSpec as P
+from jax.lax import all_to_all, axis_size
 
 norm_eps = 1e-06
 group_eps = 0.00064
@@ -126,7 +127,10 @@
     )
     partial_out = jnp.dot(
         head_out,
-        lax.all_gather(w_out, "ep", axis=1, tiled=True),
+        jnp.concatenate(
+            all_to_all(jnp.stack([w_out for _ in range(axis_size("ep"))], axis=0), "ep", 0, 0),
+            axis=1,
+        ),
         preferred_element_type=jnp.float32,
     )
     mixed_out = taken_together(partial_out.astype(jnp.bfloat16), "tp").astype(jnp.float32)

time: 268 us -> 226 us (0.84)
  waiting for transfers between devices: 154 us -> 91.1 us
  starting transfers between devices: 9.82 us -> 28.6 us
    all_gather x1 -> x0, waiting for transfers between devices: 54.1 us -> none  [body(): lax.all_gather(w_out, 'ep', axis=1, tiled=True)]
    all_to_all x0 -> x1, starting transfers between devices: none -> 18.9 us  [body(): all_to_all(jnp.stack([w_out for _ in range(axis_size('ep'))], axis=0), 'e...]
    all_gather x1, waiting for transfers between devices: 80.8 us -> 72.8 us  [sent_together(): out = lax.all_gather(both, axis, axis=dim, tiled=True)]
  transfers between devices with their start and end apart: 4 -> 4, of which waited for: 4 -> 3; matrix products, arithmetic and copies ran while one was open for 14% -> 16% of each run, Pallas kernels for 0% -> 0%
where the time goes in v1:
time: 226 us; the launch traced here: 225 us
  waiting for transfers between devices  91.1 us (40%)
  blocking collectives  43.8 us (19%)
  starting transfers between devices  28.6 us (13%)
  local copies, waits for them, and re-layouts  19.7 us (9%)
  other arithmetic  17.3 us (8%)
  between operations  14.4 us (6%)
  matrix products  10.6 us (5%)
    all_gather x1, waiting for transfers between devices, sent_together(): out = lax.all_gather(both, axis, axis=dim, tiled=True)  72.8 us
    all_to_all x1, blocking collectives, body(): lax.all_to_all(outbound, 'ep', split_axis=0, concat_axis=0, tiled=True)  31.6 us
    all_to_all x1, starting transfers between devices, body(): all_to_all(jnp.stack([w_out for _ in range(axis_size('ep'))], axis=0), 'e...  18.9 us
    all_to_all x1, waiting for transfers between devices, body(): lax.all_to_all(reduced.astype(jnp.bfloat16), 'ep', split_axis=0, concat_a...  12.8 us
    all_to_all x1, blocking collectives, sum_at_owner(): parts = lax.all_to_all(split_up(array, dim, peers), axis, 0, 0, tiled=True)  12.2 us
    mul x1, other arithmetic, recurrence(): removed[:, :, :, None] * (unit_keys * rate_heads)[:, :, None, :]  8.83 us
    all_to_all x1, starting transfers between devices, body(): lax.all_to_all(reduced.astype(jnp.bfloat16), 'ep', split_axis=0, concat_a...  5.77 us
    all_to_all x1, waiting for transfers between devices, from_everyone(): return lax.all_to_all(copies, axis, split_axis=0, concat_axis=0, tiled=True)  5.47 us
  transfers between devices with their start and end apart: 4, of which 3 were waited for; matrix products, arithmetic and copies ran while one was open for 16% of the time, Pallas kernels for 0%

profile of v1, /device:TPU:1, one launch (start us, length us, event | category | flops | bytes accessed | tf_op | source)
XLA Modules:
  0.0 225.5 jit_solution(3566104951445410757)
XLA Ops:
  7.3 1.4 pad_maximum_fusion
  8.7 1.8 stack.2
  10.5 18.9 %all-to-all-start = ((bf16[128,256,16]{1,2,0:T(8,128)(2,1)}), bf16[128,256,16]{1,2,0:T(8,128)(2,1)}, u32[]{:S(2)}, u32[]{:S(2)}) async-start(bf16[128,256,16]{1,2,0:T(8,128)(2,1)} %stack.2), calls=%async_computation | async-start | bytes 2097152 | tf_op jit(solution)/shard_map/all_to_all | solution.py:131
  29.4 0.1 fusion.34
  29.5 1.1 fusion.10
  30.8 1.2 fusion.55
  32.0 2.1 reshape.164
  34.2 1.5 mul.214
  35.7 3.0 %mul.234 = f32[16,4,4096]{2,1,0:T(4,128)} reshape(f32[16,4,64,64]{3,2,1,0:T(8,128)} %mul.214) | data formatting | bytes 2097152 | tf_op jit(solution)/shard_map/mul | solution.py:69
  38.9 0.1 eq.28
  39.2 72.8 %all-gather.2.cloned.1.call-done = bf16[2048,768]{1,0:T(8,128)(2,1)} async-done(((bf16[16,768]{1,0:T(8,128)(2,1)}), bf16[2048,768]{1,0:T(8,128)(2,1)}) %all-gather.2.cloned.1.call-update) | async-done | bytes 3145744 | tf_op jit(solution)/shard_map/all_gather | solution.py:14
  111.9 1.5 fusion.14
  113.4 0.1 reshape.175
  113.5 1.5 fusion.12
  115.1 1.5 fusion.13
  116.7 0.1 multiply_reduce_fusion.4
  116.9 8.8 %broadcast_multiply_fusion = (f32[16,4,64,64]{3,2,1,0:T(8,128)}, f32[16,4,64]{2,1,0:T(4,128)S(1)}, f32[16,4,64,64]{3,2,1,0:T(8,128)}) fusion(f32[16,4,64]{2,1,0:T(4,128)S(1)} %reshape.175, f32[16,4,64]{2,1,0:T(4,128)S(1)} %reshape.176, f32[16,4,64]{2,1,0:T(4,128)S(1)} %reshape.177, f32[16,4,64,64]{3,2,1,0:T(8,128)S(1)} %reshape.164, ...), kind=kOutput, calls=%fused_computation.33 | output fusion | flops 2097215 | bytes 3260416 | tf_op jit(solution)/shard_map/mul | solution.py:70
  125.8 3.2 %mul.236 = f32[16,4,4096]{2,1,0:T(4,128)} reshape(f32[16,4,64,64]{3,2,1,0:T(8,128)} %get-tuple-element.12) | data formatting | bytes 2097152 | tf_op jit(solution)/shard_map/mul | solution.py:70
  128.9 1.8 mul.237
  130.8 0.1 mul.232
  130.9 1.8 mul.238
  132.7 4.1 %multiply_reduce_fusion.2 = (f32[16,4]{1,0:T(8,128)S(1)}, f32[16,4,4096]{2,1,0:T(4,128)}) fusion(f32[16,4,4096]{2,1,0:T(4,128)} %mul.238, f32[16,4,4096]{2,1,0:T(4,128)} %mul.237, f32[16,4,4096]{2,1,0:T(4,128)} %mul.236, f32[16,4,4096]{2,1,0:T(4,128)} %param.20, f32[16,4,4096]{2,1,0:T(4,128)} %mul.234), kind=kLoop, calls=%fused_computation.31 | loop fusion | flops 1310656 | bytes 6291712 | tf_op jit(solution)/shard_map/reduce_sum | solution.py:74
  136.8 0.2 multiply_reduce_fusion.3
  137.0 0.1 multiply_convert_fusion
  137.1 0.1 convert_element_type.88
  137.2 1.6 convolution_convert_fusion.2
  138.8 0.7 broadcast_in_dim.2
  139.5 4.0 %all-to-all-start.1 = ((bf16[4,16,2048]{2,1,0:T(8,128)(2,1)}), bf16[4,16,2048]{2,1,0:T(8,128)(2,1)S(1)}, u32[]{:S(2)}, u32[]{:S(2)}) async-start(bf16[4,16,2048]{2,1,0:T(8,128)(2,1)} %broadcast_in_dim.2), calls=%async_computation.1 | async-start | bytes 524288 | tf_op jit(solution)/shard_map/all_to_all | solution.py:20
  143.5 0.2 select_reduce_fusion.1
  143.9 5.5 %all-to-all-done.1 = bf16[4,16,2048]{2,1,0:T(8,128)(2,1)S(1)} async-done(((bf16[4,16,2048]{2,1,0:T(8,128)(2,1)}), bf16[4,16,2048]{2,1,0:T(8,128)(2,1)S(1)}, u32[]{:S(2)}, u32[]{:S(2)}) %all-to-all-start.1) | async-done | bytes 262176 | tf_op jit(solution)/shard_map/all_to_all | solution.py:20
  149.5 0.1 fusion.31
  149.6 0.3 fusion.1
  149.9 0.5 broadcast.136
  150.5 1.0 reduce.4
  151.5 0.4 reshape.179
  151.9 31.6 %all_to_all.25 = bf16[128,2,1024]{2,1,0:T(2,128)(2,1)S(1)} all-to-all(bf16[128,2,1024]{2,1,0:T(2,128)(2,1)S(1)} %reshape.179), channel_id=1, replica_groups=mesh['ep'=128,'tp'=4] {'ep'}, dimensions={0} | all-to-all | bytes 1048576 | tf_op jit(solution)/shard_map/all_to_all | solution.py:154
  183.4 0.4 reshape.180
  183.9 0.4 fusion.22
  184.3 0.7 convolution_convert_fusion
  185.0 0.4 reshape.172
  185.4 0.1 copy.86
  185.5 12.2 %all_to_all.26 = bf16[4,128,1,512]{3,1,2,0:T(8,128)(2,1)S(1)} all-to-all(bf16[4,128,1,512]{3,1,2,0:T(8,128)(2,1)S(1)} %bitcast.42), channel_id=1, replica_groups=mesh['ep'=128,'tp'=4] {'tp'}, dimensions={0} | all-to-all | bytes 1048576 | tf_op jit(solution)/shard_map/all_to_all | solution.py:35
  197.8 0.7 reduce.5
  198.5 0.7 reshape.181
  199.2 5.8 %all-to-all-start.4 = ((bf16[128,2,256]{2,1,0:T(2,128)(2,1)}), bf16[128,2,256]{2,1,0:T(2,128)(2,1)S(1)}, u32[]{:S(2)}, u32[]{:S(2)}) async-start(bf16[128,2,256]{2,1,0:T(2,128)(2,1)} %reshape.181), calls=%async_computation.4 | async-start | bytes 262144 | tf_op jit(solution)/shard_map/all_to_all | solution.py:164
  205.0 12.8 %all-to-all-done.4 = bf16[128,2,256]{2,1,0:T(2,128)(2,1)S(1)} async-done(((bf16[128,2,256]{2,1,0:T(2,128)(2,1)}), bf16[128,2,256]{2,1,0:T(2,128)(2,1)S(1)}, u32[]{:S(2)}, u32[]{:S(2)}) %all-to-all-start.4) | async-done | bytes 131104 | tf_op jit(solution)/shard_map/all_to_all | solution.py:164
  217.8 0.1 reshape.182
  217.9 0.8 fusion.7
  (51 shorter events, 1.3 us)
Async XLA Ops:
  7.2 177.2 %copy-start = (bf16[1,128,2048]{2,1,0:T(8,128)(2,1)S(1)}, bf16[1,128,2048]{2,1,0:T(8,128)(2,1)}, u32[]{:S(2)}) copy-start(bf16[1,128,2048]{2,1,0:T(8,128)(2,1)} %param.37) | copy-start | bytes 1572868
  7.2 22.2 %copy-start.2 = (bf16[16,2048]{1,0:T(8,128)(2,1)S(1)}, bf16[16,2048]{1,0:T(8,128)(2,1)}, u32[]{:S(2)}) copy-start(bf16[16,2048]{1,0:T(8,128)(2,1)} %param.19) | copy-start | bytes 196612
  7.2 22.3 %copy-start.7 = (f32[2048]{0:T(1024)S(1)}, f32[2048]{0:T(1024)}, u32[]{:S(2)}) copy-start(f32[2048]{0:T(1024)} %param.21) | copy-start | bytes 24580
  7.2 22.3 %copy-start.5 = (bf16[2048,64]{0,1:T(8,128)(2,1)S(1)}, bf16[2048,64]{0,1:T(8,128)(2,1)}, u32[]{:S(2)}) copy-start(bf16[2048,64]{0,1:T(8,128)(2,1)} %param.28) | copy-start | bytes 786436
  7.2 23.6 %copy-start.6 = (bf16[2048,64]{0,1:T(8,128)(2,1)S(1)}, bf16[2048,64]{0,1:T(8,128)(2,1)}, u32[]{:S(2)}) copy-start(bf16[2048,64]{0,1:T(8,128)(2,1)} %param.25) | copy-start | bytes 786436
  7.2 23.6 %copy-start.11 = (f32[256]{0:T(256)S(1)}, f32[256]{0:T(256)}, u32[]{:S(2)}) copy-start(f32[256]{0:T(256)} %param.27) | copy-start | bytes 3076
  7.2 104.7 %all-gather.2.cloned.1.call-start = ((), (), s32[]{:S(2)}) async-start(), calls=%async_computation.5 | async-start | bytes 3170304 | tf_op jit(solution)/shard_map/all_gather | solution.py:14
  10.5 126.7 %all-to-all-start = ((bf16[128,256,16]{1,2,0:T(8,128)(2,1)}), bf16[128,256,16]{1,2,0:T(8,128)(2,1)}, u32[]{:S(2)}, u32[]{:S(2)}) async-start(bf16[128,256,16]{1,2,0:T(8,128)(2,1)} %stack.2), calls=%async_computation | async-start | bytes 2097152 | tf_op jit(solution)/shard_map/all_to_all | solution.py:131
  35.7 3.1 %copy-start.12 = (f32[256]{0:T(256)S(1)}, f32[256]{0:T(256)}, u32[]{:S(2)}) copy-start(f32[256]{0:T(256)} %param.30) | copy-start | bytes 3076
  35.7 3.1 %copy-start.9 = (s32[16,2]{0,1:T(2,128)S(1)}, s32[16,2]{0,1:T(2,128)}, u32[]{:S(2)}) copy-start(s32[16,2]{0,1:T(2,128)} %param.33) | copy-start | bytes 388
  35.7 3.4 %copy-start.10 = (f32[16,2]{0,1:T(2,128)S(1)}, f32[16,2]{0,1:T(2,128)}, u32[]{:S(2)}) copy-start(f32[16,2]{0,1:T(2,128)} %param.34) | copy-start | bytes 388
  125.8 3.2 %copy-start.1 = (f32[16,4,64,64]{3,2,1,0:T(8,128)S(1)}, f32[16,4,64,64]{3,2,1,0:T(8,128)}, u32[]{:S(2)}) copy-start(f32[16,4,64,64]{3,2,1,0:T(8,128)} %get-tuple-element.10) | copy-start | bytes 3145732
  136.8 12.8 %copy-start.8 = (f32[2048]{0:T(1024)S(1)}, f32[2048]{0:T(1024)}, u32[]{:S(2)}) copy-start(f32[2048]{0:T(1024)} %param.32) | copy-start | bytes 24580
  139.5 9.9 %all-to-all-start.1 = ((bf16[4,16,2048]{2,1,0:T(8,128)(2,1)}), bf16[4,16,2048]{2,1,0:T(8,128)(2,1)S(1)}, u32[]{:S(2)}, u32[]{:S(2)}) async-start(bf16[4,16,2048]{2,1,0:T(8,128)(2,1)} %broadcast_in_dim.2), calls=%async_computation.1 | async-start | bytes 524288 | tf_op jit(solution)/shard_map/all_to_all | solution.py:20
  151.5 32.4 %copy-start.3 = (bf16[1,2048,128]{2,1,0:T(8,128)(2,1)S(1)}, bf16[1,2048,128]{2,1,0:T(8,128)(2,1)}, u32[]{:S(2)}) copy-start(bf16[1,2048,128]{2,1,0:T(8,128)(2,1)} %param.35) | copy-start | bytes 1572868
  151.8 32.5 %copy-start.4 = (bf16[1,2048,128]{2,1,0:T(8,128)(2,1)S(1)}, bf16[1,2048,128]{2,1,0:T(8,128)(2,1)}, u32[]{:S(2)}) copy-start(bf16[1,2048,128]{2,1,0:T(8,128)(2,1)} %param.36) | copy-start | bytes 1572868
  199.2 18.6 %all-to-all-start.4 = ((bf16[128,2,256]{2,1,0:T(2,128)(2,1)}), bf16[128,2,256]{2,1,0:T(2,128)(2,1)S(1)}, u32[]{:S(2)}, u32[]{:S(2)}) async-start(bf16[128,2,256]{2,1,0:T(2,128)(2,1)} %reshape.181), calls=%async_computation.4 | async-start | bytes 262144 | tf_op jit(solution)/shard_map/all_to_all | solution.py:164
Sparse Core Ops, SparseCore 0:
  11.7 100.1 all-gather.1
